TPU v7x, 32 devices: a whole 2x2x4 slice. The times are simulated.
32 devices in a mesh: ep: 8 (over z, core), tp: 4 (over y, x).
Axes of the slice: x: 2, y: 2, z: 4, core: 2. Of those that a mesh axis runs over, the one named last changes fastest.
Arguments:
- probe_preactivations: bfloat16 [4096, 2048], P('ep', 'tp'), may hold values from -6 to 6
- rightward_retain_scores: bfloat16 [4096, 2048], P('ep', 'tp'), may hold values from -5.5 to 5.5
- leftward_retain_scores: bfloat16 [4096, 2048], P('ep', 'tp'), may hold values from -5.5 to 5.5
- payload_vectors: bfloat16 [4096, 2048], P('ep', 'tp'), may hold values from -6 to 6
- retain_minimum_bounds: float32 [2, 2048], P(None, 'tp'), may hold values from 0.88 to 1
- extra_shrink_spikes: float32 [16, 4096], P('tp', 'ep'), may hold values from -0.7 to 0
- mixer_rescale_factor: float32 [2048], P('tp'), may hold values from 0.1 to 1.9
- mixer_emit_matrix: bfloat16 [2048, 2048], P('tp'), may hold values from -0.1875 to 0.1875
- specialist_arriving_tokens: bfloat16 [1024, 2048], P('ep'), may hold values from -6 to 6
- specialist_rescale_factor: float32 [2048], replicated, may hold values from 0.1 to 1.9
- routed_specialist_ids: int32 [1024, 2], P('ep'), may hold values from 0 to 7, all different within a row; in each aligned block of 128 rows (0 to 127, 128 to 255, ...) at most 64 rows name the same one
- routed_specialist_shares: float32 [1024, 2], P('ep'), may hold values from 0.1 to 1
- specialist_switch_matrix: bfloat16 [8, 2048, 3584], P('ep', None, 'tp'), may hold values from -0.125 to 0.125
- specialist_widen_matrix: bfloat16 [8, 2048, 3584], P('ep', None, 'tp'), may hold values from -0.125 to 0.125
- specialist_shrink_matrix: bfloat16 [8, 3584, 2048], P('ep', 'tp'), may hold values from -0.125 to 0.125
Outputs:
- mixed_a: bfloat16 [4096, 2048], P('ep', 'tp')
- mixed_b: bfloat16 [1024, 2048], P('ep', 'tp')
Inputs may be any that keep to these rules, and one draw needn't show every extreme that they name: `routed_specialist_ids`: each row names 2 different experts; within the rows of one index of ep no expert is named by more than 64 rows, and in every draw some expert is named by exactly 64 rows of some index.
All inputs are finite; a program needn't handle non-finite values.
Results may differ from a plain program's by a relative error of at most 0.015.
Values may be sent and summed in bfloat16 or wider, within the bound.
A program may use at most 64 MiB of HBM per device.

v0:
```python
import jax
import jax.numpy as jnp
from jax import lax
from jax.experimental import pallas as pl
from jax.experimental.pallas import tpu as pltpu
from jax.sharding import PartitionSpec as P

DK = 128
CHUNK = 128
PAD = 16
EPS = 1e-06

NT = (((1,), (1,)), ((), ()))
TN = (((0,), (0,)), ((), ()))


def params(count):
    return pltpu.CompilerParams(dimension_semantics=("arbitrary",) * count)


def cost(flops, moved):
    return pl.CostEstimate(flops=flops, bytes_accessed=moved, transcendentals=0)


def dot(a, b, dims=(((1,), (0,)), ((), ()))):
    return lax.dot_general(a, b, dims, preferred_element_type=jnp.float32)


def split(x):
    high = x.astype(jnp.bfloat16)
    return high, (x - high.astype(jnp.float32)).astype(jnp.bfloat16)


def states_kernel(xf_ref, xb_ref, v_ref, bound_ref, spike_ref, cf_ref, eb_ref, state_ref):
    length, width = xf_ref.shape
    head = pl.program_id(0)
    bound_f = bound_ref[0:1, :]
    bound_b = bound_ref[1:2, :]
    spike = jnp.broadcast_to(spike_ref[pl.ds(head, 1), :], (width, length)).T
    row = lax.broadcasted_iota(jnp.int32, (CHUNK, CHUNK), 0)
    col = lax.broadcasted_iota(jnp.int32, (CHUNK, CHUNK), 1)
    tri = (row >= col).astype(jnp.bfloat16)
    carry_f = jnp.zeros((1, width), jnp.float32)
    carry_b = jnp.zeros((1, width), jnp.float32)
    keys_f, keys_b, cums_f = [], [], []
    for at in range(0, length, CHUNK):
        rows = slice(at, at + CHUNK)
        xf = xf_ref[rows, :].astype(jnp.float32)
        xb = xb_ref[rows, :].astype(jnp.float32)
        lf = jnp.log(bound_f + (1.0 - bound_f) * jax.nn.sigmoid(xf)) + spike[rows]
        lb = jnp.log(bound_b + (1.0 - bound_b) * jax.nn.sigmoid(xb)) + spike[rows]
        summed = dot(tri, jnp.concatenate([*split(lf), *split(lb)], axis=1))
        cf = carry_f + summed[:, :width] + summed[:, width : 2 * width]
        cb = carry_b + summed[:, 2 * width : 3 * width] + summed[:, 3 * width :]
        carry_f = cf[CHUNK - 1 :]
        carry_b = cb[CHUNK - 1 :]
        eb = cb - lb
        cf_ref[rows, :] = cf
        eb_ref[rows, :] = eb
        cums_f.append(cf)
        keys_f.append((1.0 - bound_f) * jax.nn.sigmoid(-xf))
        keys_b.append(((1.0 - bound_b) * jax.nn.sigmoid(-xb) * jnp.exp(eb)).astype(jnp.bfloat16))
    eb_ref[length:, :] = jnp.broadcast_to(carry_b, (8, width))
    keys_f = [(k * jnp.exp(carry_f - c)).astype(jnp.bfloat16) for k, c in zip(keys_f, cums_f)]
    v = v_ref[...]
    for way, (keys, total) in enumerate(((keys_f, carry_f), (keys_b, carry_b))):
        state = dot(v, jnp.concatenate(keys, axis=0), TN)
        high, low = split(jnp.broadcast_to(total, (PAD // 2, width)))
        state_ref[way, 0, :DK, :] = state.astype(jnp.bfloat16)
        state_ref[way, 0, DK:, :] = jnp.concatenate(
            [high.astype(jnp.float32), low.astype(jnp.float32)], axis=0
        ).astype(jnp.bfloat16)


def local_kernel(q_ref, xf_ref, xb_ref, v_ref, bound_ref, cf_ref, eb_ref, o_ref, qf_ref, qb_ref):
    length, width = xf_ref.shape
    bound_f = bound_ref[0:1, :]
    bound_b = bound_ref[1:2, :]
    row = lax.broadcasted_iota(jnp.int32, (CHUNK, CHUNK), 0)
    col = lax.broadcasted_iota(jnp.int32, (CHUNK, CHUNK), 1)
    total_b = eb_ref[length : length + 1, :]
    count = length // CHUNK
    bf = jnp.bfloat16
    later, outs = [], []
    state = None
    for c in range(count):
        at = c * CHUNK
        rows = slice(at, at + CHUNK)
        half = at + CHUNK // 2
        q = q_ref[rows, :].astype(jnp.float32)
        q = q * jax.nn.sigmoid(q)
        v = v_ref[rows, :]
        cf = cf_ref[rows, :]
        eb = eb_ref[rows, :]
        mid_f = cf_ref[half : half + 1, :]
        mid_b = eb_ref[half : half + 1, :]
        end_f = cf[CHUNK - 1 :]
        end_b = eb_ref[at + CHUNK : at + CHUNK + 1, :]
        kf = (1.0 - bound_f) * jax.nn.sigmoid(-xf_ref[rows, :].astype(jnp.float32))
        kb = (1.0 - bound_b) * jax.nn.sigmoid(-xb_ref[rows, :].astype(jnp.float32))
        q_f = q * jnp.exp(cf - mid_f)
        k_f = kf * jnp.exp(mid_f - cf)
        q_b = q * jnp.exp(mid_b - eb)
        k_b = kb * jnp.exp(eb - mid_b)
        scores = jnp.where(row >= col, dot(q_f.astype(bf), k_f.astype(bf), NT), 0.0)
        scores += jnp.where(row <= col, dot(q_b.astype(bf), k_b.astype(bf), NT), 0.0)
        out = dot(scores.astype(bf), v)
        qf_ref[rows, :] = (q_f * jnp.exp(mid_f)).astype(bf)
        qb_ref[rows, :] = (q_b * jnp.exp(total_b - mid_b)).astype(bf)
        base_f = cf_ref[at - 1 : at, :] if c else None
        if c:
            out += dot((q_f * jnp.exp(mid_f - base_f)).astype(bf), state.astype(bf), NT)
        if c < count - 1:
            gained = dot(v, (k_f * jnp.exp(end_f - mid_f)).astype(bf), TN)
            state = state * jnp.exp(end_f - base_f) + gained if c else gained
        start_b = eb[:1]
        into = (q_b * jnp.exp(end_b - mid_b)).astype(bf) if c < count - 1 else None
        gained_b = dot(v, (k_b * jnp.exp(mid_b - start_b)).astype(bf), TN) if c else None
        later.append((into, gained_b, end_b - start_b))
        outs.append(out)
    state = None
    for c in reversed(range(count)):
        into, gained_b, span = later[c]
        out = outs[c]
        if state is not None:
            out += dot(into, state.astype(bf), NT)
        o_ref[c * CHUNK : (c + 1) * CHUNK, :] = out
        if c:
            state = gained_b if state is None else state * jnp.exp(span) + gained_b


def join_kernel(place_ref, o_ref, qf_ref, qb_ref, all_ref, gain_ref, mixed_ref):
    place = place_ref[0]
    peers = all_ref.shape[0]
    width = o_ref.shape[1]

    def part(at, way):
        state = all_ref[at, way, 0, :DK, :].astype(jnp.float32)
        totals = all_ref[at, way, 0, DK:, :].astype(jnp.float32)
        return state, jnp.exp(totals[:1] + totals[PAD // 2 : PAD // 2 + 1])

    def forward(at, acc):
        state, decay = part(at, 0)
        return acc * decay + state

    def backward(k, acc):
        state, decay = part(peers - 1 - k, 1)
        return acc * decay + state

    zero = jnp.zeros((DK, width), jnp.float32)
    entry_f = lax.fori_loop(0, place, forward, zero).astype(jnp.bfloat16)
    entry_b = lax.fori_loop(0, peers - 1 - place, backward, zero).astype(jnp.bfloat16)
    out = o_ref[...] + dot(qf_ref[...], entry_f, NT) + dot(qb_ref[...], entry_b, NT)
    scale = lax.rsqrt(jnp.mean(out * out, axis=-1, keepdims=True) + EPS)
    mixed_ref[...] = (out * scale * gain_ref[...]).astype(jnp.bfloat16)


def partial_kernel(x_ref, w_ref, o_ref):
    o_ref[0] = dot(x_ref[...], w_ref[...]).astype(jnp.bfloat16)


def grouped(x, w, groups):
    rows, depth = x.shape
    cols = w.shape[1] // groups
    return pl.pallas_call(
        partial_kernel,
        grid=(groups,),
        in_specs=[
            pl.BlockSpec((rows, depth), lambda g: (0, 0)),
            pl.BlockSpec((depth, cols), lambda g: (0, g)),
        ],
        out_specs=pl.BlockSpec((1, rows, cols), lambda g: (g, 0, 0)),
        out_shape=jax.ShapeDtypeStruct((groups, rows, cols), jnp.bfloat16),
        compiler_params=params(1),
        cost_estimate=cost(2 * rows * depth * w.shape[1], 2 * (x.size + w.size + rows * w.shape[1])),
    )(x, w)


def per_device(
    probe_preactivations,
    rightward_retain_scores,
    leftward_retain_scores,
    payload_vectors,
    retain_minimum_bounds,
    extra_shrink_spikes,
    mixer_rescale_factor,
    mixer_emit_matrix,
    specialist_arriving_tokens,
    specialist_rescale_factor,
    routed_specialist_ids,
    routed_specialist_shares,
    specialist_switch_matrix,
    specialist_widen_matrix,
    specialist_shrink_matrix,
):
    peers = lax.axis_size("ep")
    groups = lax.axis_size("tp")
    length, width = probe_preactivations.shape
    heads = width // DK

    rows_b, features = specialist_arriving_tokens.shape
    picks = routed_specialist_ids.shape[1]
    capacity = 2 * rows_b * picks // peers
    slots = peers * capacity
    rows_f = specialist_arriving_tokens.astype(jnp.float32)
    normed_b = (
        rows_f
        * lax.rsqrt(jnp.mean(rows_f * rows_f, axis=-1, keepdims=True) + EPS)
        * specialist_rescale_factor
    ).astype(jnp.bfloat16)
    flat_ids = routed_specialist_ids.reshape(-1)
    number = jnp.arange(rows_b * picks, dtype=jnp.int32)
    same = (flat_ids[:, None] == flat_ids[None, :]) & (number[None, :] < number[:, None])
    ranking = jnp.sum(same.astype(jnp.int32), axis=1)
    slot_of = (flat_ids * capacity + ranking).reshape(rows_b, picks)
    slot_grid = jnp.arange(slots, dtype=jnp.int32)
    hits = slot_of[:, :, None] == slot_grid[None, None, :]
    pick_matrix = jnp.any(hits, axis=1).astype(jnp.bfloat16)
    share_matrix = jnp.sum(jnp.where(hits, routed_specialist_shares[:, :, None], 0.0), axis=1)
    outgoing = dot(pick_matrix, normed_b, TN).astype(jnp.bfloat16)
    arrived = lax.all_to_all(
        outgoing.reshape(peers, capacity, features), "ep", split_axis=0, concat_axis=0, tiled=True
    )

    tile = pl.BlockSpec((length, DK), lambda h: (0, h))
    tall = pl.BlockSpec((length + 8, DK), lambda h: (0, h))
    bound_tile = pl.BlockSpec((2, DK), lambda h: (0, h))
    wide = jax.ShapeDtypeStruct((length, width), jnp.float32)
    narrow = jax.ShapeDtypeStruct((length, width), jnp.bfloat16)
    cum_f, cum_b, states = pl.pallas_call(
        states_kernel,
        grid=(heads,),
        in_specs=[tile, tile, tile, bound_tile, pl.BlockSpec((heads, length), lambda h: (0, 0))],
        out_specs=[tile, tall, pl.BlockSpec((2, 1, DK + PAD, DK), lambda h: (0, h, 0, 0))],
        out_shape=[
            wide,
            jax.ShapeDtypeStruct((length + 8, width), jnp.float32),
            jax.ShapeDtypeStruct((2, heads, DK + PAD, DK), jnp.bfloat16),
        ],
        compiler_params=params(1),
        cost_estimate=cost(4 * 10**9, 16 * length * width),
    )(
        rightward_retain_scores,
        leftward_retain_scores,
        payload_vectors,
        retain_minimum_bounds,
        extra_shrink_spikes,
    )
    everything = lax.all_gather(states, "ep")
    local_out, query_f, query_b = pl.pallas_call(
        local_kernel,
        grid=(heads,),
        in_specs=[tile, tile, tile, tile, bound_tile, tile, tall],
        out_specs=[tile, tile, tile],
        out_shape=[wide, narrow, narrow],
        compiler_params=params(1),
        cost_estimate=cost(8 * 10**9, 24 * length * width),
    )(
        probe_preactivations,
        rightward_retain_scores,
        leftward_retain_scores,
        payload_vectors,
        retain_minimum_bounds,
        cum_f,
        cum_b,
    )

    arrived = arrived.reshape(slots, features)
    gate_out = dot(arrived, specialist_switch_matrix[0])
    up_out = dot(arrived, specialist_widen_matrix[0])
    hidden = (jax.nn.silu(gate_out) * up_out).astype(jnp.bfloat16)
    expert_part = grouped(hidden, specialist_shrink_matrix[0], groups)
    expert_total = lax.psum_scatter(expert_part, "tp", scatter_dimension=0, tiled=True)

    mixed_heads = pl.pallas_call(
        join_kernel,
        grid=(heads,),
        in_specs=[
            pl.BlockSpec(memory_space=pltpu.SMEM),
            tile,
            tile,
            tile,
            pl.BlockSpec((peers, 2, 1, DK + PAD, DK), lambda h: (0, 0, h, 0, 0)),
            pl.BlockSpec((1, DK), lambda h: (0, h)),
        ],
        out_specs=tile,
        out_shape=narrow,
        compiler_params=params(1),
        cost_estimate=cost(2 * 10**9, 10 * length * width),
    )(
        lax.axis_index("ep").reshape(1),
        local_out,
        query_f,
        query_b,
        everything,
        mixer_rescale_factor.reshape(1, -1),
    )
    mixer_part = grouped(mixed_heads, mixer_emit_matrix, groups)
    mixed_a = lax.psum_scatter(mixer_part, "tp", scatter_dimension=0, tiled=True)

    returned = lax.all_to_all(
        expert_total.reshape(peers, capacity, -1), "ep", split_axis=0, concat_axis=0, tiled=True
    ).reshape(slots, -1)
    share_high, share_low = split(share_matrix)
    mixed_b = (dot(share_high, returned) + dot(share_low, returned)).astype(jnp.bfloat16)
    return mixed_a.reshape(length, -1), mixed_b


def solution(mesh):
    in_specs = (
        P("ep", "tp"),
        P("ep", "tp"),
        P("ep", "tp"),
        P("ep", "tp"),
        P(None, "tp"),
        P("tp", "ep"),
        P("tp"),
        P("tp", None),
        P("ep", None),
        P(),
        P("ep", None),
        P("ep", None),
        P("ep", None, "tp"),
        P("ep", None, "tp"),
        P("ep", "tp", None),
    )
    out_specs = (P("ep", "tp"), P("ep", "tp"))
    return jax.shard_map(
        per_device, mesh=mesh, in_specs=in_specs, out_specs=out_specs, check_vma=False
    )
```

profile of v0, /device:TPU:0, one launch (start us, length us, event | category | flops | bytes accessed | tf_op | source)
XLA Modules:
  0.0 182.8 jit_solution(990247227635574899)
XLA Ops:
  8.0 1.2 fusion.7
  9.2 0.8 copy.31
  10.0 0.1 eq.28
  10.2 0.2 convert_reduce_fusion
  10.3 0.1 reduce_sum.30
  10.5 0.1 copy.32
  10.6 0.7 multiply_add_fusion
  11.3 0.1 fusion.13
  11.4 3.2 %convolution_convert_fusion = bf16[512,2048]{1,0:T(8,128)(2,1)} fusion(pred[128,512]{1,0:T(8,128)(4,1)S(1)} %fusion.13, bf16[128,2048]{1,0:T(8,128)(2,1)} %param.23, f32[2048]{0:T(1024)} %param.24, f32[128]{0:T(128)S(1)} %add_rsqrt_fusion), kind=kOutput, calls=%fused_computation.4 | convolution fusion | flops 270532608 | bytes 2695680 | tf_op jit(solution)/shard_map/dot_general | solution.py:26
  14.6 6.3 %all-to-all-start = ((bf16[8,64,2048]{2,1,0:T(8,128)(2,1)}), bf16[8,64,2048]{2,1,0:T(8,128)(2,1)S(1)}, u32[]{:S(2)}, u32[]{:S(2)}) async-start(bf16[8,64,2048]{2,1,0:T(8,128)(2,1)} %bitcast.4), calls=%async_computation | async-start | bytes 4194304 | tf_op jit(solution)/shard_map/all_to_all | solution.py:221
  20.9 0.0 all-gather.3.cloned.1.call-start
  21.0 5.0 %shard_map.158 = (f32[512,512]{1,0:T(8,128)}, f32[520,512]{1,0:T(8,128)}, bf16[2,4,144,128]{3,2,1,0:T(8,128)(2,1)}) custom-call(bf16[512,512]{1,0:T(8,128)(2,1)} %xf_ref.3, bf16[512,512]{1,0:T(8,128)(2,1)} %xb_ref.3, bf16[512,512]{1,0:T(8,128)(2,1)} %v_ref.3, f32[2,512]{1,0:T(2,128)} %bound_ref.3, f32[4,512]{1,0:T(4,128)} %spike_ref.1), custom_call_target="tpu_custom_call" | custom-call | flops 4000000000 | bytes 4194304 | tf_op jit(solution)/shard_map/pallas_call | solution.py:230
  26.0 0.0 all-gather.3.cloned.1.call-update
  26.0 0.0 reduce-scatter.9.cloned.1.call-start
  26.1 62.8 %all-to-all-done = bf16[8,64,2048]{2,1,0:T(8,128)(2,1)S(1)} async-done(((bf16[8,64,2048]{2,1,0:T(8,128)(2,1)}), bf16[8,64,2048]{2,1,0:T(8,128)(2,1)S(1)}, u32[]{:S(2)}, u32[]{:S(2)}) %all-to-all-start) | async-done | bytes 2097184 | tf_op jit(solution)/shard_map/all_to_all | solution.py:221
  88.9 0.0 copy-start.1
  88.9 4.5 %fusion.2 = f32[512,896]{1,0:T(8,128)S(1)} fusion(bf16[512,2048]{1,0:T(8,128)(2,1)S(1)} %bitcast.25, bf16[1,2048,896]{2,1,0:T(8,128)(2,1)} %param.27), kind=kOutput, calls=%fused_computation.2 | convolution fusion | flops 1879048192 | bytes 7602176 | tf_op jit(solution)/shard_map/dot_general | solution.py:26
  93.4 0.0 copy-done.1
  93.4 3.4 %multiply_convert_fusion.x_ref = bf16[512,896]{1,0:T(8,128)(2,1)} fusion(f32[512,896]{1,0:T(8,128)S(1)} %fusion.2, bf16[512,2048]{1,0:T(8,128)(2,1)S(1)} %bitcast.26, bf16[1,2048,896]{2,1,0:T(8,128)(2,1)S(1)} %copy-done.1), kind=kOutput, calls=%fused_computation.5 | convolution fusion | flops 1881800704 | bytes 8519680 | tf_op jit(solution)/shard_map/dot_general | solution.py:26
  96.8 5.9 %shard_map.162 = bf16[4,512,512]{2,1,0:T(8,128)(2,1)} custom-call(bf16[512,896]{1,0:T(8,128)(2,1)} %multiply_convert_fusion.x_ref, bf16[896,2048]{1,0:T(8,128)(2,1)} %bitcast.28), custom_call_target="tpu_custom_call" | custom-call | flops 1879048192 | bytes 6684672 | tf_op jit(solution)/shard_map/pallas_call | solution.py:165
  102.7 0.0 reduce-scatter.9.cloned.1.call-update
  102.7 0.0 reduce-scatter.7.cloned.1.call-start
  102.8 6.1 %shard_map.159 = (f32[512,512]{1,0:T(8,128)}, bf16[512,512]{1,0:T(8,128)(2,1)}, bf16[512,512]{1,0:T(8,128)(2,1)}) custom-call(bf16[512,512]{1,0:T(8,128)(2,1)} %q_ref.1, bf16[512,512]{1,0:T(8,128)(2,1)} %xf_ref.3, bf16[512,512]{1,0:T(8,128)(2,1)} %xb_ref.3, bf16[512,512]{1,0:T(8,128)(2,1)} %v_ref.3, f32[2,512]{1,0:T(2,128)} %bound_ref.3, ...), custom_call_target="tpu_custom_call" | custom-call | flops 8000000000 | bytes 6291456 | tf_op jit(solution)/shard_map/pallas_call | solution.py:250
  108.9 0.0 all-gather.3.cloned.1.call-done
  108.9 4.9 %shard_map.160.x_ref = bf16[512,512]{1,0:T(8,128)(2,1)} custom-call(s32[1]{0:T(128)} %bitcast.place_ref, f32[512,512]{1,0:T(8,128)} %get-tuple-element.10.o_ref, bf16[512,512]{1,0:T(8,128)(2,1)} %get-tuple-element.11.qf_ref, bf16[512,512]{1,0:T(8,128)(2,1)} %get-tuple-element.12.qb_ref, bf16[8,2,4,144,128]{4,3,2,1,0:T(8,128)(2,1)} %bitcast.29, f32[1,512]{1,0:T(1,128)} %bitcast.31), custom_call_target="tpu_custom_call" | custom-call | flops 2000000000 | bytes 2621440 | tf_op jit(solution)/shard_map/pallas_call | solution.py:275
  113.8 4.8 %shard_map.161 = bf16[4,512,512]{2,1,0:T(8,128)(2,1)} custom-call(bf16[512,512]{1,0:T(8,128)(2,1)} %shard_map.160.x_ref, bf16[512,2048]{1,0:T(8,128)(2,1)} %w_ref.1), custom_call_target="tpu_custom_call" | custom-call | flops 1073741824 | bytes 4718592 | tf_op jit(solution)/shard_map/pallas_call | solution.py:165
  118.6 0.0 copy-start
  118.6 0.0 reduce-scatter.7.cloned.1.call-update
  118.7 18.2 %reduce-scatter.9.cloned.1.call-done = bf16[1,512,512]{2,1,0:T(8,128)(2,1)} async-done(((bf16[4,512,512]{2,1,0:T(8,128)(2,1)}), bf16[1,512,512]{2,1,0:T(8,128)(2,1)}) %reduce-scatter.9.cloned.1.call-update) | async-done | bytes 524304
  136.9 4.6 %all-to-all-start.1 = ((bf16[8,64,512]{2,1,0:T(8,128)(2,1)}), bf16[8,64,512]{2,1,0:T(8,128)(2,1)S(1)}, u32[]{:S(2)}, u32[]{:S(2)}) async-start(bf16[8,64,512]{2,1,0:T(8,128)(2,1)} %bitcast.27), calls=%async_computation.1 | async-start | bytes 1048576 | tf_op jit(solution)/shard_map/all_to_all | solution.py:301
  141.5 0.0 copy-done
  141.5 0.1 select_reduce_fusion
  141.6 15.2 %all-to-all-done.1 = bf16[8,64,512]{2,1,0:T(8,128)(2,1)S(1)} async-done(((bf16[8,64,512]{2,1,0:T(8,128)(2,1)}), bf16[8,64,512]{2,1,0:T(8,128)(2,1)S(1)}, u32[]{:S(2)}, u32[]{:S(2)}) %all-to-all-start.1) | async-done | bytes 524320 | tf_op jit(solution)/shard_map/all_to_all | solution.py:301
  156.8 0.2 fusion.16
  157.0 0.9 fusion.6
  157.9 17.5 %reduce-scatter.7.cloned.1.call-done = bf16[1,512,512]{2,1,0:T(8,128)(2,1)} async-done(((bf16[4,512,512]{2,1,0:T(8,128)(2,1)}), bf16[1,512,512]{2,1,0:T(8,128)(2,1)}) %reduce-scatter.7.cloned.1.call-update) | async-done | bytes 524304
  (1 shorter events, 0.0 us)
Async XLA Ops:
  14.6 74.3 %all-to-all-start = ((bf16[8,64,2048]{2,1,0:T(8,128)(2,1)}), bf16[8,64,2048]{2,1,0:T(8,128)(2,1)S(1)}, u32[]{:S(2)}, u32[]{:S(2)}) async-start(bf16[8,64,2048]{2,1,0:T(8,128)(2,1)} %bitcast.4), calls=%async_computation | async-start | bytes 4194304 | tf_op jit(solution)/shard_map/all_to_all | solution.py:221
  20.9 88.0 %all-gather.3.cloned.1.call-start = ((), (), s32[]{:S(2)}) async-start(), calls=%async_computation.4 | async-start | bytes 2654208 | tf_op jit(solution)/shard_map/all_gather | solution.py:249
  26.0 110.9 %reduce-scatter.9.cloned.1.call-start = ((), (), s32[]{:S(2)}) async-start(), calls=%async_computation.6 | async-start | bytes 2621440
  88.9 4.5 %copy-start.1 = (bf16[1,2048,896]{2,1,0:T(8,128)(2,1)S(1)}, bf16[1,2048,896]{2,1,0:T(8,128)(2,1)}, u32[]{:S(2)}) copy-start(bf16[1,2048,896]{2,1,0:T(8,128)(2,1)} %param.28) | copy-start | bytes 11010052
  102.7 72.7 %reduce-scatter.7.cloned.1.call-start = ((), (), s32[]{:S(2)}) async-start(), calls=%async_computation.5 | async-start | bytes 2621440
  118.6 22.9 %copy-start = (f32[128,2]{0,1:T(2,128)S(1)}, f32[128,2]{0,1:T(2,128)}, u32[]{:S(2)}) copy-start(f32[128,2]{0,1:T(2,128)} %param.26) | copy-start | bytes 3076
  136.9 19.9 %all-to-all-start.1 = ((bf16[8,64,512]{2,1,0:T(8,128)(2,1)}), bf16[8,64,512]{2,1,0:T(8,128)(2,1)S(1)}, u32[]{:S(2)}, u32[]{:S(2)}) async-start(bf16[8,64,512]{2,1,0:T(8,128)(2,1)} %bitcast.27), calls=%async_computation.1 | async-start | bytes 1048576 | tf_op jit(solution)/shard_map/all_to_all | solution.py:301
Sparse Core Ops, SparseCore 0:
  26.1 58.3 all-gather.2
Sparse Core Ops, SparseCore 1:
  102.8 34.0 reduce-scatter.8
  140.3 35.1 reduce-scatter.6
where the time goes:
time: 184 us; the launch traced here: 183 us
  waiting for transfers between devices  114 us (62%)
  Pallas kernels  26.7 us (15%)
  between operations  15.5 us (8%)
  matrix products  12.2 us (7%)
  starting transfers between devices  11.1 us (6%)
  other arithmetic  2.38 us (1%)
    all_to_all x1, waiting for transfers between devices, per_device(): lax.all_to_all(outgoing.reshape(peers, capacity, features), 'ep', split_a...  62.8 us
    unnamed x5, waiting for transfers between devices  35.7 us
    all_to_all x1, waiting for transfers between devices, per_device(): lax.all_to_all(expert_total.reshape(peers, capacity, -1), 'ep', split_axi...  15.2 us
    dot_general x5, matrix products, dot(): return lax.dot_general(a, b, dims, preferred_element_type=jnp.float32)  12.2 us
    pallas_call x2, Pallas kernels, grouped(): pl.pallas_call(partial_kernel, grid=(groups,), in_specs=[pl.BlockSpec((ro...  10.6 us
    all_to_all x1, starting transfers between devices, per_device(): lax.all_to_all(outgoing.reshape(peers, capacity, features), 'ep', split_a...  6.35 us
    pallas_call x1, Pallas kernels, per_device(): pl.pallas_call(local_kernel, grid=(heads,), in_specs=[tile, tile, tile, t...  6.15 us
    pallas_call x1, Pallas kernels, per_device(): pl.pallas_call(states_kernel, grid=(heads,), in_specs=[tile, tile, tile,...  5.03 us
  transfers between devices with their start and end apart: 5, of which 4 were waited for; matrix products, arithmetic and copies ran while one was open for 5% of the time, Pallas kernels for 15%

commit v1 on v0

v1 whole, which is shorter than its diff:
```python
import jax
import jax.numpy as jnp
from jax import lax
from jax.experimental import pallas as pl
from jax.experimental.pallas import tpu as pltpu
from jax.sharding import PartitionSpec as P

DK = 128
CHUNK = 128
EPS = 1e-06
MESH = pl.DeviceIdType.MESH
VMEM_LIMIT = 48 * 2**20

NT = (((1,), (1,)), ((), ()))
TN = (((0,), (0,)), ((), ()))


def cost(flops, moved):
    return pl.CostEstimate(flops=flops, bytes_accessed=moved, transcendentals=0)


def dot(a, b, dims=(((1,), (0,)), ((), ()))):
    return lax.dot_general(a, b, dims, preferred_element_type=jnp.float32)


def split(x):
    high = x.astype(jnp.bfloat16)
    return high, (x - high.astype(jnp.float32)).astype(jnp.bfloat16)


def states_of(xf_ref, xb_ref, v_ref, bound_ref, spike_ref, cf_ref, eb_ref, state_ref, total_ref):
    length, width = xf_ref.shape
    bound_f = bound_ref[0:1, :]
    bound_b = bound_ref[1:2, :]
    spike = jnp.broadcast_to(spike_ref[...], (width, length)).T
    row = lax.broadcasted_iota(jnp.int32, (CHUNK, CHUNK), 0)
    col = lax.broadcasted_iota(jnp.int32, (CHUNK, CHUNK), 1)
    tri = (row >= col).astype(jnp.bfloat16)
    carry_f = jnp.zeros((1, width), jnp.float32)
    carry_b = jnp.zeros((1, width), jnp.float32)
    keys_f, keys_b, cums_f = [], [], []
    for at in range(0, length, CHUNK):
        rows = slice(at, at + CHUNK)
        xf = xf_ref[rows, :].astype(jnp.float32)
        xb = xb_ref[rows, :].astype(jnp.float32)
        lf = jnp.log(bound_f + (1.0 - bound_f) * jax.nn.sigmoid(xf)) + spike[rows]
        lb = jnp.log(bound_b + (1.0 - bound_b) * jax.nn.sigmoid(xb)) + spike[rows]
        summed = dot(tri, jnp.concatenate([*split(lf), *split(lb)], axis=1))
        cf = carry_f + summed[:, :width] + summed[:, width : 2 * width]
        cb = carry_b + summed[:, 2 * width : 3 * width] + summed[:, 3 * width :]
        carry_f = cf[CHUNK - 1 :]
        carry_b = cb[CHUNK - 1 :]
        eb = cb - lb
        cf_ref[rows, :] = cf
        eb_ref[rows, :] = eb
        cums_f.append(cf)
        keys_f.append((1.0 - bound_f) * jax.nn.sigmoid(-xf))
        keys_b.append(((1.0 - bound_b) * jax.nn.sigmoid(-xb) * jnp.exp(eb)).astype(jnp.bfloat16))
    eb_ref[length:, :] = jnp.broadcast_to(carry_b, (8, width))
    keys_f = [(k * jnp.exp(carry_f - c)).astype(jnp.bfloat16) for k, c in zip(keys_f, cums_f)]
    v = v_ref[...]
    for way, (keys, total) in enumerate(((keys_f, carry_f), (keys_b, carry_b))):
        state_ref[way] = dot(v, jnp.concatenate(keys, axis=0), TN)
        total_ref[way] = jnp.broadcast_to(total, (8, width))


def local_of(q_ref, xf_ref, xb_ref, v_ref, bound_ref, cf_ref, eb_ref, o_ref, qf_ref, qb_ref):
    length, width = xf_ref.shape
    bound_f = bound_ref[0:1, :]
    bound_b = bound_ref[1:2, :]
    row = lax.broadcasted_iota(jnp.int32, (CHUNK, CHUNK), 0)
    col = lax.broadcasted_iota(jnp.int32, (CHUNK, CHUNK), 1)
    total_b = eb_ref[length : length + 1, :]
    count = length // CHUNK
    bf = jnp.bfloat16
    later, outs = [], []
    state = None
    for c in range(count):
        at = c * CHUNK
        rows = slice(at, at + CHUNK)
        half = at + CHUNK // 2
        q = q_ref[rows, :].astype(jnp.float32)
        q = q * jax.nn.sigmoid(q)
        v = v_ref[rows, :]
        cf = cf_ref[rows, :]
        eb = eb_ref[rows, :]
        mid_f = cf_ref[half : half + 1, :]
        mid_b = eb_ref[half : half + 1, :]
        end_f = cf[CHUNK - 1 :]
        end_b = eb_ref[at + CHUNK : at + CHUNK + 1, :]
        kf = (1.0 - bound_f) * jax.nn.sigmoid(-xf_ref[rows, :].astype(jnp.float32))
        kb = (1.0 - bound_b) * jax.nn.sigmoid(-xb_ref[rows, :].astype(jnp.float32))
        q_f = q * jnp.exp(cf - mid_f)
        k_f = kf * jnp.exp(mid_f - cf)
        q_b = q * jnp.exp(mid_b - eb)
        k_b = kb * jnp.exp(eb - mid_b)
        scores = jnp.where(row >= col, dot(q_f.astype(bf), k_f.astype(bf), NT), 0.0)
        scores += jnp.where(row <= col, dot(q_b.astype(bf), k_b.astype(bf), NT), 0.0)
        out = dot(scores.astype(bf), v)
        qf_ref[rows, :] = (q_f * jnp.exp(mid_f)).astype(bf)
        qb_ref[rows, :] = (q_b * jnp.exp(total_b - mid_b)).astype(bf)
        base_f = cf_ref[at - 1 : at, :] if c else None
        if c:
            out += dot((q_f * jnp.exp(mid_f - base_f)).astype(bf), state.astype(bf), NT)
        if c < count - 1:
            gained = dot(v, (k_f * jnp.exp(end_f - mid_f)).astype(bf), TN)
            state = state * jnp.exp(end_f - base_f) + gained if c else gained
        start_b = eb[:1]
        into = (q_b * jnp.exp(end_b - mid_b)).astype(bf) if c < count - 1 else None
        gained_b = dot(v, (k_b * jnp.exp(mid_b - start_b)).astype(bf), TN) if c else None
        later.append((into, gained_b, end_b - start_b))
        outs.append(out)
    state = None
    for c in reversed(range(count)):
        into, gained_b, span = later[c]
        out = outs[c]
        if state is not None:
            out += dot(into, state.astype(bf), NT)
        o_ref[c * CHUNK : (c + 1) * CHUNK, :] = out
        if c:
            state = gained_b if state is None else state * jnp.exp(span) + gained_b


def greet(axis):
    count = lax.axis_size(axis)
    me = lax.axis_index(axis)
    barrier = pltpu.get_barrier_semaphore()

    def one(k, carry):
        pl.semaphore_signal(barrier, inc=1, device_id={axis: lax.rem(me + k, count)}, device_id_type=MESH)
        return carry

    lax.fori_loop(1, count, one, 0)
    return count - 1


def sent(source, target, send, recv, axis, peer):
    return pltpu.make_async_remote_copy(
        src_ref=source,
        dst_ref=target,
        send_sem=send,
        recv_sem=recv,
        device_id={axis: peer},
        device_id_type=MESH,
    )


def head_kernel(
    q_ref,
    xf_ref,
    xb_ref,
    v_ref,
    bound_ref,
    spike_ref,
    gain_ref,
    outgoing_ref,
    arrived_ref,
    mixed_ref,
    cf_ref,
    eb_ref,
    local_ref,
    qf_ref,
    qb_ref,
    state_ref,
    total_ref,
    chain_out,
    chain_in,
    far_send,
    far_recv,
    near_send,
    near_recv,
    chain_send,
    chain_recv,
):
    peers, groups = lax.axis_size("ep"), lax.axis_size("tp")
    place, group = lax.axis_index("ep"), lax.axis_index("tp")
    heads = state_ref.shape[0]
    share = outgoing_ref.shape[2] // groups
    ours = pl.ds(pl.multiple_of(group * share, share), share)
    waits = greet("ep") + greet("tp")
    pl.semaphore_wait(pltpu.get_barrier_semaphore(), waits)

    far = []
    for k in range(1, peers):
        peer = lax.rem(place + k, peers)
        copy = sent(
            outgoing_ref.at[peer, :, ours],
            arrived_ref.at[place, :, ours],
            far_send.at[k - 1],
            far_recv.at[k - 1],
            "ep",
            peer,
        )
        copy.start()
        far.append(copy)
    arrived_ref[place] = outgoing_ref[place]

    def lanes(h):
        return pl.ds(pl.multiple_of(h * DK, DK), DK)

    def states_step(h, carry):
        at = lanes(h)
        states_of(
            xf_ref.at[:, at],
            xb_ref.at[:, at],
            v_ref.at[:, at],
            bound_ref.at[:, at],
            spike_ref.at[pl.ds(h, 1), :],
            cf_ref.at[h],
            eb_ref.at[h],
            state_ref.at[h],
            total_ref.at[h],
        )
        return carry

    lax.fori_loop(0, heads, states_step, 0)

    near = []
    for k in range(1, peers):
        far[k - 1].wait_recv()
        source = lax.rem(place + peers - k, peers)
        for j in range(1, groups):
            block = arrived_ref.at[source, :, ours]
            copy = sent(
                block,
                block,
                near_send.at[k - 1, j - 1],
                near_recv.at[k - 1, j - 1],
                "tp",
                lax.rem(group + j, groups),
            )
            copy.start()
            near.append(copy)

    def local_step(h, carry):
        at = lanes(h)
        local_of(
            q_ref.at[:, at],
            xf_ref.at[:, at],
            xb_ref.at[:, at],
            v_ref.at[:, at],
            bound_ref.at[:, at],
            cf_ref.at[h],
            eb_ref.at[h],
            local_ref.at[h],
            qf_ref.at[h],
            qb_ref.at[h],
        )
        return carry

    lax.fori_loop(0, heads, local_step, 0)

    def chain(way):
        first, last = (0, peers - 1) if way == 0 else (peers - 1, 0)
        to = lax.rem(place + (1 if way == 0 else peers - 1), peers)
        copy = sent(
            chain_out.at[way], chain_in.at[way], chain_send.at[way], chain_recv.at[way], "ep", to
        )

        def advance():
            @pl.when(place != first)
            def _():
                copy.wait_recv()

            @pl.when(place == first)
            def _():
                chain_in[way] = jnp.zeros(chain_in.shape[1:], jnp.bfloat16)

            @pl.when(place != last)
            def _():
                for h in range(heads):
                    decay = jnp.exp(total_ref[h, way][:1])
                    chain_out[way, h] = (
                        chain_in[way, h].astype(jnp.float32) * decay + state_ref[h, way]
                    ).astype(jnp.bfloat16)
                copy.start()

        def finish():
            @pl.when(place != last)
            def _():
                copy.wait_send()

        return advance, finish

    advance_f, finish_f = chain(0)
    advance_b, finish_b = chain(1)

    @pl.when(2 * place < peers)
    def _():
        advance_f()
        advance_b()

    @pl.when(2 * place >= peers)
    def _():
        advance_b()
        advance_f()

    def join_step(h, carry):
        at = lanes(h)
        out = local_ref[h] + dot(qf_ref[h], chain_in[0, h], NT) + dot(qb_ref[h], chain_in[1, h], NT)
        scale = lax.rsqrt(jnp.mean(out * out, axis=-1, keepdims=True) + EPS)
        mixed_ref[:, at] = (out * scale * gain_ref[:, at]).astype(jnp.bfloat16)
        return carry

    lax.fori_loop(0, heads, join_step, 0)
    finish_f()
    finish_b()
    for copy in far:
        copy.wait_send()
    for copy in near:
        copy.wait()


def tail_kernel(
    hidden_ref,
    down_ref,
    mixed_ref,
    emit_ref,
    high_ref,
    low_ref,
    out_a_ref,
    out_b_ref,
    part_b,
    got_b,
    part_a,
    got_a,
    total_b,
    returned,
    send_b,
    recv_b,
    send_a,
    recv_a,
    back_send,
    back_recv,
):
    peers, groups = lax.axis_size("ep"), lax.axis_size("tp")
    place, group = lax.axis_index("ep"), lax.axis_index("tp")
    cols = part_a.shape[2]
    waits = greet("ep") + greet("tp")
    pl.semaphore_wait(pltpu.get_barrier_semaphore(), waits)

    def scatter(x_ref, w_ref, part, got, send, recv):
        copies = []
        for k in range(1, groups + 1):
            peer = lax.rem(group + k, groups)
            at = pl.ds(pl.multiple_of(peer * cols, cols), cols)
            part[k - 1] = dot(x_ref[...], w_ref[:, at]).astype(jnp.bfloat16)
            if k < groups:
                copy = sent(part.at[k - 1], got.at[k - 1], send.at[k - 1], recv.at[k - 1], "tp", peer)
                copy.start()
                copies.append(copy)
        return copies

    def total(part, got, copies):
        for copy in copies:
            copy.wait_recv()
        value = part[groups - 1].astype(jnp.float32)
        for k in range(groups - 1):
            value += got[k].astype(jnp.float32)
        return value.astype(jnp.bfloat16)

    copies_b = scatter(hidden_ref, down_ref, part_b, got_b, send_b, recv_b)
    copies_a = scatter(mixed_ref, emit_ref, part_a, got_a, send_a, recv_a)
    total_b[...] = total(part_b, got_b, copies_b).reshape(total_b.shape)
    back = []
    for k in range(1, peers):
        peer = lax.rem(place + k, peers)
        copy = sent(
            total_b.at[peer], returned.at[place], back_send.at[k - 1], back_recv.at[k - 1], "ep", peer
        )
        copy.start()
        back.append(copy)
    returned[place] = total_b[place]
    out_a_ref[...] = total(part_a, got_a, copies_a)
    for copy in back:
        copy.wait_recv()
    rows = returned[...].reshape(-1, cols)
    out_b_ref[...] = (dot(high_ref[...], rows) + dot(low_ref[...], rows)).astype(jnp.bfloat16)
    for copy in copies_b + copies_a + back:
        copy.wait_send()


def per_device(
    probe_preactivations,
    rightward_retain_scores,
    leftward_retain_scores,
    payload_vectors,
    retain_minimum_bounds,
    extra_shrink_spikes,
    mixer_rescale_factor,
    mixer_emit_matrix,
    specialist_arriving_tokens,
    specialist_rescale_factor,
    routed_specialist_ids,
    routed_specialist_shares,
    specialist_switch_matrix,
    specialist_widen_matrix,
    specialist_shrink_matrix,
):
    peers = lax.axis_size("ep")
    groups = lax.axis_size("tp")
    length, width = probe_preactivations.shape
    heads = width // DK

    rows_b, features = specialist_arriving_tokens.shape
    picks = routed_specialist_ids.shape[1]
    capacity = 2 * rows_b * picks // peers
    slots = peers * capacity
    rows_f = specialist_arriving_tokens.astype(jnp.float32)
    normed_b = (
        rows_f
        * lax.rsqrt(jnp.mean(rows_f * rows_f, axis=-1, keepdims=True) + EPS)
        * specialist_rescale_factor
    ).astype(jnp.bfloat16)
    flat_ids = routed_specialist_ids.reshape(-1)
    number = jnp.arange(rows_b * picks, dtype=jnp.int32)
    same = (flat_ids[:, None] == flat_ids[None, :]) & (number[None, :] < number[:, None])
    ranking = jnp.sum(same.astype(jnp.int32), axis=1)
    slot_of = (flat_ids * capacity + ranking).reshape(rows_b, picks)
    slot_grid = jnp.arange(slots, dtype=jnp.int32)
    hits = slot_of[:, :, None] == slot_grid[None, None, :]
    pick_matrix = jnp.any(hits, axis=1).astype(jnp.bfloat16)
    share_matrix = jnp.sum(jnp.where(hits, routed_specialist_shares[:, :, None], 0.0), axis=1)
    outgoing = dot(pick_matrix, normed_b, TN).astype(jnp.bfloat16)
    vmem = pl.BlockSpec(memory_space=pltpu.VMEM)
    dma = pltpu.SemaphoreType.DMA
    bf, f32 = jnp.bfloat16, jnp.float32
    arrived, mixed_heads = pl.pallas_call(
        head_kernel,
        in_specs=[vmem] * 8,
        out_specs=[vmem] * 2,
        out_shape=[
            jax.ShapeDtypeStruct((peers, capacity, features), bf),
            jax.ShapeDtypeStruct((length, width), bf),
        ],
        scratch_shapes=[
            pltpu.VMEM((heads, length, DK), f32),
            pltpu.VMEM((heads, length + 8, DK), f32),
            pltpu.VMEM((heads, length, DK), f32),
            pltpu.VMEM((heads, length, DK), bf),
            pltpu.VMEM((heads, length, DK), bf),
            pltpu.VMEM((heads, 2, DK, DK), f32),
            pltpu.VMEM((heads, 2, 8, DK), f32),
            pltpu.VMEM((2, heads, DK, DK), bf),
            pltpu.VMEM((2, heads, DK, DK), bf),
            dma((peers - 1,)),
            dma((peers - 1,)),
            dma((peers - 1, groups - 1)),
            dma((peers - 1, groups - 1)),
            dma((2,)),
            dma((2,)),
        ],
        compiler_params=pltpu.CompilerParams(
            collective_id=0, has_side_effects=True, vmem_limit_bytes=VMEM_LIMIT
        ),
        cost_estimate=cost(2 * 10**10, 10**7),
    )(
        probe_preactivations,
        rightward_retain_scores,
        leftward_retain_scores,
        payload_vectors,
        retain_minimum_bounds,
        extra_shrink_spikes,
        mixer_rescale_factor.reshape(1, -1),
        outgoing.reshape(peers, capacity, features),
    )

    arrived = arrived.reshape(slots, features)
    gate_out = dot(arrived, specialist_switch_matrix[0])
    up_out = dot(arrived, specialist_widen_matrix[0])
    hidden = (jax.nn.silu(gate_out) * up_out).astype(bf)

    share_high, share_low = split(share_matrix)
    cols = features // groups
    cols_a = mixer_emit_matrix.shape[1] // groups
    return tuple(
        pl.pallas_call(
            tail_kernel,
            in_specs=[vmem] * 6,
            out_specs=[vmem] * 2,
            out_shape=[
                jax.ShapeDtypeStruct((length, cols_a), bf),
                jax.ShapeDtypeStruct((rows_b, cols), bf),
            ],
            scratch_shapes=[
                pltpu.VMEM((groups, slots, cols), bf),
                pltpu.VMEM((groups - 1, slots, cols), bf),
                pltpu.VMEM((groups, length, cols_a), bf),
                pltpu.VMEM((groups - 1, length, cols_a), bf),
                pltpu.VMEM((peers, capacity, cols), bf),
                pltpu.VMEM((peers, capacity, cols), bf),
                dma((groups - 1,)),
                dma((groups - 1,)),
                dma((groups - 1,)),
                dma((groups - 1,)),
                dma((peers - 1,)),
                dma((peers - 1,)),
            ],
            compiler_params=pltpu.CompilerParams(
                collective_id=1, has_side_effects=True, vmem_limit_bytes=VMEM_LIMIT
            ),
            cost_estimate=cost(2 * 10**10, 10**7),
        )(
            hidden,
            specialist_shrink_matrix[0],
            mixed_heads,
            mixer_emit_matrix,
            share_high,
            share_low,
        )
    )


def solution(mesh):
    in_specs = (
        P("ep", "tp"),
        P("ep", "tp"),
        P("ep", "tp"),
        P("ep", "tp"),
        P(None, "tp"),
        P("tp", "ep"),
        P("tp"),
        P("tp", None),
        P("ep", None),
        P(),
        P("ep", None),
        P("ep", None),
        P("ep", None, "tp"),
        P("ep", None, "tp"),
        P("ep", "tp", None),
    )
    out_specs = (P("ep", "tp"), P("ep", "tp"))
    return jax.shard_map(
        per_device, mesh=mesh, in_specs=in_specs, out_specs=out_specs, check_vma=False
    )
```

time: 184 us -> 107 us (0.58)
  waiting for transfers between devices: 114 us -> 0 us
  Pallas kernels: 26.7 us -> 92.6 us
  between operations: 15.5 us -> 0.85 us
  starting transfers between devices: 11.1 us -> 0 us
  matrix products: 12.2 us -> 7.94 us
    all_to_all x2 -> x0, waiting for transfers between devices: 78 us -> none  [the longest x1 62.8 us: per_device(): lax.all_to_all(outgoing.reshape(peers, capacity, features), 'ep', split_a...]
    pallas_call x5 -> x2, Pallas kernels: 26.7 us -> 92.6 us  [the longest x1 52.1 us: per_device(): pl.pallas_call(tail_kernel, in_specs=[vmem] * 6, out_specs=[vmem] * 2, ou...]
    unnamed x5 -> x0, waiting for transfers between devices: 35.7 us -> none
    all_to_all x2 -> x0, starting transfers between devices: 11 us -> none  [the longest x1 6.35 us: per_device(): lax.all_to_all(outgoing.reshape(peers, capacity, features), 'ep', split_a...]
    dot_general x5 -> x3, matrix products: 12.2 us -> 7.94 us  [dot(): return lax.dot_general(a, b, dims, preferred_element_type=jnp.float32)]
  transfers between devices with their start and end apart: 5 -> 0, of which waited for: 4 -> 0; matrix products, arithmetic and copies ran while one was open for 5% -> 0% of each run, Pallas kernels for 15% -> 0%
where the time goes in v1:
time: 107 us
  Pallas kernels  92.6 us (87%)
  matrix products  7.94 us (7%)
  local copies, waits for them, and re-layouts  2.77 us (3%)
  other arithmetic  2.4 us (2%)
    pallas_call x1, Pallas kernels, per_device(): pl.pallas_call(tail_kernel, in_specs=[vmem] * 6, out_specs=[vmem] * 2, ou...  52.1 us
    pallas_call x1, Pallas kernels, per_device(): pl.pallas_call(head_kernel, in_specs=[vmem] * 8, out_specs=[vmem] * 2, ou...  40.5 us
    dot_general x3, matrix products, dot(): return lax.dot_general(a, b, dims, preferred_element_type=jnp.float32)  7.94 us
    unnamed x25, local copies, waits for them, and re-layouts  2.43 us

profile of v1, /device:TPU:0, one launch (start us, length us, event | category | flops | bytes accessed | tf_op | source)
XLA Modules:
  0.0 106.6 jit_solution(8208833302833540541)
XLA Ops:
  0.6 0.0 copy-start.7
  0.6 0.0 copy-start.1
  0.7 0.0 copy-start.2
  0.7 0.0 copy-start.3
  0.7 0.0 copy-start.4
  0.7 0.0 copy-start.6
  0.7 0.0 copy-start.5
  0.7 0.9 copy.27
  1.6 0.1 eq.28
  1.8 0.2 convert_reduce_fusion
  2.0 0.1 reduce_sum.30
  2.1 0.1 copy.28
  2.2 0.7 multiply_add_fusion
  2.9 0.1 fusion.12
  3.0 1.2 %fusion.6 = f32[128]{0:T(128)S(1)} fusion(bf16[128,2048]{1,0:T(8,128)(2,1)} %param.23), kind=kLoop, calls=%fused_computation.8 | loop fusion | flops 786304 | bytes 524800 | tf_op jit(solution)/shard_map/reduce_sum | solution.py:412
  4.2 3.2 %convolution_convert_fusion = bf16[512,2048]{1,0:T(8,128)(2,1)} fusion(pred[128,512]{1,0:T(8,128)(4,1)S(1)} %fusion.12, bf16[128,2048]{1,0:T(8,128)(2,1)} %param.23, f32[2048]{0:T(1024)} %param.24, f32[128]{0:T(128)S(1)} %add_rsqrt_fusion), kind=kOutput, calls=%fused_computation.4 | convolution fusion | flops 270532608 | bytes 2695680 | tf_op jit(solution)/shard_map/dot_general | solution.py:23
  7.4 0.0 copy-done.7
  7.4 0.0 copy-done.1
  7.4 0.0 copy-done.2
  7.4 0.0 copy-done.3
  7.4 0.0 copy-done.4
  7.5 0.0 copy-done.6
  7.5 0.0 copy-done.5
  7.5 0.0 copy-start.9
  7.5 40.5 %shard_map.158 = (bf16[8,64,2048]{2,1,0:T(8,128)(2,1)S(1)}, bf16[512,512]{1,0:T(8,128)(2,1)S(1)}) custom-call(bf16[512,512]{1,0:T(8,128)(2,1)S(1)} %copy-done.1, bf16[512,512]{1,0:T(8,128)(2,1)S(1)} %copy-done.2, bf16[512,512]{1,0:T(8,128)(2,1)S(1)} %copy-done.3, bf16[512,512]{1,0:T(8,128)(2,1)S(1)} %copy-done.4, f32[2,512]{1,0:T(2,128)S(1)} %copy-done.6, ...), custom_call_target="tpu_custom_call" | custom-call | flops 20000000000 | bytes 10000000 | tf_op jit(solution)/shard_map/pallas_call | solution.py:428
  48.0 0.0 copy-done.9
  48.0 0.0 copy-start.10
  48.0 2.3 %fusion.2 = f32[512,896]{1,0:T(8,128)S(1)} fusion(bf16[512,2048]{1,0:T(8,128)(2,1)S(1)} %bitcast.16, bf16[1,2048,896]{2,1,0:T(8,128)(2,1)S(1)} %copy-done.9), kind=kOutput, calls=%fused_computation.2 | convolution fusion | flops 1879048192 | bytes 7602176 | tf_op jit(solution)/shard_map/dot_general | solution.py:23
  50.3 0.0 copy-done.10
  50.4 0.0 copy-start.8
  50.4 0.0 copy-start
  50.4 2.4 %multiply_convert_fusion.hidden_ref = bf16[512,896]{1,0:T(8,128)(2,1)S(1)} fusion(f32[512,896]{1,0:T(8,128)S(1)} %fusion.2, bf16[512,2048]{1,0:T(8,128)(2,1)S(1)} %bitcast.17, bf16[1,2048,896]{2,1,0:T(8,128)(2,1)S(1)} %copy-done.10), kind=kOutput, calls=%fused_computation.5 | convolution fusion | flops 1881800704 | bytes 8519680 | tf_op jit(solution)/shard_map/dot_general | solution.py:23
  52.8 0.0 copy-done.8
  52.8 0.1 select_reduce_fusion
  53.0 0.0 copy-done
  53.0 52.1 %shard_map.159 = (bf16[512,512]{1,0:T(8,128)(2,1)S(1)}, bf16[128,512]{1,0:T(8,128)(2,1)S(1)}) custom-call(bf16[512,896]{1,0:T(8,128)(2,1)S(1)} %multiply_convert_fusion.hidden_ref, bf16[896,2048]{1,0:T(8,128)(2,1)} %bitcast.19, bf16[512,512]{1,0:T(8,128)(2,1)S(1)} %get-tuple-element.5.mixed_ref, bf16[512,2048]{1,0:T(8,128)(2,1)S(1)} %copy-done, ...), custom_call_target="tpu_custom_call" | custom-call | flops 20000000000 | bytes 10000000 | tf_op jit(solution)/shard_map/pallas_call | solution.py:477
  105.1 0.8 copy.31
  105.9 0.7 copy.32
  (2 shorter events, 0.0 us)
Async XLA Ops:
  0.6 6.8 %copy-start.7 = (f32[512]{0:T(512)S(1)}, f32[512]{0:T(512)}, u32[]{:S(2)}) copy-start(f32[512]{0:T(512)} %param.21) | copy-start | bytes 6148
  0.6 6.8 %copy-start.1 = (bf16[512,512]{1,0:T(8,128)(2,1)S(1)}, bf16[512,512]{1,0:T(8,128)(2,1)}, u32[]{:S(2)}) copy-start(bf16[512,512]{1,0:T(8,128)(2,1)} %q_ref.1) | copy-start | bytes 1572868
  0.7 6.8 %copy-start.2 = (bf16[512,512]{1,0:T(8,128)(2,1)S(1)}, bf16[512,512]{1,0:T(8,128)(2,1)}, u32[]{:S(2)}) copy-start(bf16[512,512]{1,0:T(8,128)(2,1)} %xf_ref.1) | copy-start | bytes 1572868
  0.7 6.8 %copy-start.3 = (bf16[512,512]{1,0:T(8,128)(2,1)S(1)}, bf16[512,512]{1,0:T(8,128)(2,1)}, u32[]{:S(2)}) copy-start(bf16[512,512]{1,0:T(8,128)(2,1)} %xb_ref.1) | copy-start | bytes 1572868
  0.7 6.8 %copy-start.4 = (bf16[512,512]{1,0:T(8,128)(2,1)S(1)}, bf16[512,512]{1,0:T(8,128)(2,1)}, u32[]{:S(2)}) copy-start(bf16[512,512]{1,0:T(8,128)(2,1)} %v_ref.1) | copy-start | bytes 1572868
  0.7 6.8 %copy-start.6 = (f32[2,512]{1,0:T(2,128)S(1)}, f32[2,512]{1,0:T(2,128)}, u32[]{:S(2)}) copy-start(f32[2,512]{1,0:T(2,128)} %bound_ref.1) | copy-start | bytes 12292
  0.7 6.8 %copy-start.5 = (f32[4,512]{1,0:T(4,128)S(1)}, f32[4,512]{1,0:T(4,128)}, u32[]{:S(2)}) copy-start(f32[4,512]{1,0:T(4,128)} %spike_ref.1) | copy-start | bytes 24580
  7.5 40.5 %copy-start.9 = (bf16[1,2048,896]{2,1,0:T(8,128)(2,1)S(1)}, bf16[1,2048,896]{2,1,0:T(8,128)(2,1)}, u32[]{:S(2)}) copy-start(bf16[1,2048,896]{2,1,0:T(8,128)(2,1)} %param.27) | copy-start | bytes 11010052
  48.0 2.3 %copy-start.10 = (bf16[1,2048,896]{2,1,0:T(8,128)(2,1)S(1)}, bf16[1,2048,896]{2,1,0:T(8,128)(2,1)}, u32[]{:S(2)}) copy-start(bf16[1,2048,896]{2,1,0:T(8,128)(2,1)} %param.28) | copy-start | bytes 11010052
  50.4 2.5 %copy-start.8 = (f32[128,2]{0,1:T(2,128)S(1)}, f32[128,2]{0,1:T(2,128)}, u32[]{:S(2)}) copy-start(f32[128,2]{0,1:T(2,128)} %param.26) | copy-start | bytes 3076
  50.4 2.6 %copy-start = (bf16[512,2048]{1,0:T(8,128)(2,1)S(1)}, bf16[512,2048]{1,0:T(8,128)(2,1)}, u32[]{:S(2)}) copy-start(bf16[512,2048]{1,0:T(8,128)(2,1)} %emit_ref.1) | copy-start | bytes 6291460

commit v2 on v1

--- a/solution.py
+++ b/solution.py
@@ -359,9 +359,69 @@
             value += got[k].astype(jnp.float32)
         return value.astype(jnp.bfloat16)
 
-    copies_b = scatter(hidden_ref, down_ref, part_b, got_b, send_b, recv_b)
-    copies_a = scatter(mixed_ref, emit_ref, part_a, got_a, send_a, recv_a)
-    total_b[...] = total(part_b, got_b, copies_b).reshape(total_b.shape)
+    def block(x_ref, w_ref, peer):
+        at = pl.ds(pl.multiple_of(peer * cols, cols), cols)
+        return dot(x_ref[...], w_ref[:, at]).astype(jnp.bfloat16)
+
+    side, line = lax.rem(group, 2), group // 2
+    beside, across = 2 * line + 1 - side, 2 * (1 - line) + side
+    corner = 2 * (1 - line) + 1 - side
+
+    def plan(part, got, send, recv):
+        half = part.shape[1] // 2
+        top, low = pl.ds(0, half), pl.ds(half, half)
+
+        def make(k, p, g, rows, peer):
+            return sent(part.at[p, rows], got.at[g, rows], send.at[k], recv.at[k], "tp", peer)
+
+        first = [
+            make(0, 0, 1, top, beside),
+            make(1, 0, 1, low, across),
+            make(2, 1, 0, top, beside),
+            make(3, 2, 0, low, across),
+        ]
+        second = [make(4, 2, 2, top, across), make(5, 1, 2, low, beside)]
+        return first, second
+
+    def forward(part, got, first, second):
+        half = part.shape[1] // 2
+        for copy, mine, p, rows in (
+            (second[0], first[0], 2, pl.ds(0, half)),
+            (second[1], first[1], 1, pl.ds(half, half)),
+        ):
+            mine.wait_recv()
+            summed = part[p, rows].astype(jnp.float32) + got[1, rows].astype(jnp.float32)
+            part[p, rows] = summed.astype(jnp.bfloat16)
+            copy.start()
+
+    def finish(part, got, first, second):
+        for copy in first[2:] + second:
+            copy.wait_recv()
+        value = part[3].astype(jnp.float32) + got[0].astype(jnp.float32) + got[2].astype(jnp.float32)
+        return value.astype(jnp.bfloat16)
+
+    if groups == 4:
+        plan_b = plan(part_b, got_b, send_b, recv_b)
+        plan_a = plan(part_a, got_a, send_a, recv_a)
+        part_b[0] = block(hidden_ref, down_ref, corner)
+        plan_b[0][0].start()
+        plan_b[0][1].start()
+        part_b[1] = block(hidden_ref, down_ref, beside)
+        plan_b[0][2].start()
+        part_b[2] = block(hidden_ref, down_ref, across)
+        plan_b[0][3].start()
+        part_b[3] = block(hidden_ref, down_ref, group)
+        for slot, peer in enumerate((corner, beside, across, group)):
+            part_a[slot] = block(mixed_ref, emit_ref, peer)
+        forward(part_b, got_b, *plan_b)
+        for copy in plan_a[0]:
+            copy.start()
+        copies_b, copies_a = plan_b[0] + plan_b[1], plan_a[0] + plan_a[1]
+        total_b[...] = finish(part_b, got_b, *plan_b).reshape(total_b.shape)
+    else:
+        copies_b = scatter(hidden_ref, down_ref, part_b, got_b, send_b, recv_b)
+        copies_a = scatter(mixed_ref, emit_ref, part_a, got_a, send_a, recv_a)
+        total_b[...] = total(part_b, got_b, copies_b).reshape(total_b.shape)
     back = []
     for k in range(1, peers):
         peer = lax.rem(place + k, peers)
@@ -371,7 +431,11 @@
         copy.start()
         back.append(copy)
     returned[place] = total_b[place]
-    out_a_ref[...] = total(part_a, got_a, copies_a)
+    if groups == 4:
+        forward(part_a, got_a, *plan_a)
+        out_a_ref[...] = finish(part_a, got_a, *plan_a)
+    else:
+        out_a_ref[...] = total(part_a, got_a, copies_a)
     for copy in back:
         copy.wait_recv()
     rows = returned[...].reshape(-1, cols)
@@ -489,10 +553,10 @@
                 pltpu.VMEM((groups - 1, length, cols_a), bf),
                 pltpu.VMEM((peers, capacity, cols), bf),
                 pltpu.VMEM((peers, capacity, cols), bf),
-                dma((groups - 1,)),
-                dma((groups - 1,)),
-                dma((groups - 1,)),
-                dma((groups - 1,)),
+                dma((max(groups - 1, 6),)),
+                dma((max(groups - 1, 6),)),
+                dma((max(groups - 1, 6),)),
+                dma((max(groups - 1, 6),)),
                 dma((peers - 1,)),
                 dma((peers - 1,)),
             ],

time: 107 us -> 95 us (0.89)
  Pallas kernels: 92.6 us -> 80.7 us
    pallas_call x1, Pallas kernels: 52.1 us -> 40.2 us  [per_device(): pl.pallas_call(tail_kernel, in_specs=[vmem] * 6, out_specs=[vmem] * 2, ou...]
where the time goes in v2:
time: 95 us; the launch traced here: 94.7 us
  Pallas kernels  80.7 us (85%)
  matrix products  7.94 us (8%)
  local copies, waits for them, and re-layouts  2.77 us (3%)
  other arithmetic  2.4 us (3%)
    pallas_call x1, Pallas kernels, per_device(): pl.pallas_call(head_kernel, in_specs=[vmem] * 8, out_specs=[vmem] * 2, ou...  40.5 us
    pallas_call x1, Pallas kernels, per_device(): pl.pallas_call(tail_kernel, in_specs=[vmem] * 6, out_specs=[vmem] * 2, ou...  40.2 us
    dot_general x3, matrix products, dot(): return lax.dot_general(a, b, dims, preferred_element_type=jnp.float32)  7.94 us
    unnamed x25, local copies, waits for them, and re-layouts  2.43 us

profile of v2, /device:TPU:0, one launch (start us, length us, event | category | flops | bytes accessed | tf_op | source)
XLA Modules:
  0.0 94.7 jit_solution(1533430814817944699)
XLA Ops:
  0.6 0.0 copy-start.7
  0.6 0.0 copy-start.1
  0.7 0.0 copy-start.2
  0.7 0.0 copy-start.3
  0.7 0.0 copy-start.4
  0.7 0.0 copy-start.6
  0.7 0.0 copy-start.5
  0.7 0.9 copy.27
  1.6 0.1 eq.28
  1.8 0.2 convert_reduce_fusion
  2.0 0.1 reduce_sum.30
  2.1 0.1 copy.28
  2.2 0.7 multiply_add_fusion
  2.9 0.1 fusion.12
  3.0 1.2 %fusion.6 = f32[128]{0:T(128)S(1)} fusion(bf16[128,2048]{1,0:T(8,128)(2,1)} %param.23), kind=kLoop, calls=%fused_computation.8 | loop fusion | flops 786304 | bytes 524800 | tf_op jit(solution)/shard_map/reduce_sum | solution.py:476
  4.2 3.2 %convolution_convert_fusion = bf16[512,2048]{1,0:T(8,128)(2,1)} fusion(pred[128,512]{1,0:T(8,128)(4,1)S(1)} %fusion.12, bf16[128,2048]{1,0:T(8,128)(2,1)} %param.23, f32[2048]{0:T(1024)} %param.24, f32[128]{0:T(128)S(1)} %add_rsqrt_fusion), kind=kOutput, calls=%fused_computation.4 | convolution fusion | flops 270532608 | bytes 2695680 | tf_op jit(solution)/shard_map/dot_general | solution.py:23
  7.4 0.0 copy-done.7
  7.4 0.0 copy-done.1
  7.4 0.0 copy-done.2
  7.4 0.0 copy-done.3
  7.4 0.0 copy-done.4
  7.5 0.0 copy-done.6
  7.5 0.0 copy-done.5
  7.5 0.0 copy-start.9
  7.5 40.5 %shard_map.158 = (bf16[8,64,2048]{2,1,0:T(8,128)(2,1)S(1)}, bf16[512,512]{1,0:T(8,128)(2,1)S(1)}) custom-call(bf16[512,512]{1,0:T(8,128)(2,1)S(1)} %copy-done.1, bf16[512,512]{1,0:T(8,128)(2,1)S(1)} %copy-done.2, bf16[512,512]{1,0:T(8,128)(2,1)S(1)} %copy-done.3, bf16[512,512]{1,0:T(8,128)(2,1)S(1)} %copy-done.4, f32[2,512]{1,0:T(2,128)S(1)} %copy-done.6, ...), custom_call_target="tpu_custom_call" | custom-call | flops 20000000000 | bytes 10000000 | tf_op jit(solution)/shard_map/pallas_call | solution.py:492
  48.0 0.0 copy-done.9
  48.0 0.0 copy-start.10
  48.0 2.3 %fusion.2 = f32[512,896]{1,0:T(8,128)S(1)} fusion(bf16[512,2048]{1,0:T(8,128)(2,1)S(1)} %bitcast.16, bf16[1,2048,896]{2,1,0:T(8,128)(2,1)S(1)} %copy-done.9), kind=kOutput, calls=%fused_computation.2 | convolution fusion | flops 1879048192 | bytes 7602176 | tf_op jit(solution)/shard_map/dot_general | solution.py:23
  50.3 0.0 copy-done.10
  50.4 0.0 copy-start.8
  50.4 0.0 copy-start
  50.4 2.4 %multiply_convert_fusion.hidden_ref = bf16[512,896]{1,0:T(8,128)(2,1)S(1)} fusion(f32[512,896]{1,0:T(8,128)S(1)} %fusion.2, bf16[512,2048]{1,0:T(8,128)(2,1)S(1)} %bitcast.17, bf16[1,2048,896]{2,1,0:T(8,128)(2,1)S(1)} %copy-done.10), kind=kOutput, calls=%fused_computation.5 | convolution fusion | flops 1881800704 | bytes 8519680 | tf_op jit(solution)/shard_map/dot_general | solution.py:23
  52.8 0.0 copy-done.8
  52.8 0.1 select_reduce_fusion
  53.0 0.0 copy-done
  53.0 40.2 %shard_map.159 = (bf16[512,512]{1,0:T(8,128)(2,1)S(1)}, bf16[128,512]{1,0:T(8,128)(2,1)S(1)}) custom-call(bf16[512,896]{1,0:T(8,128)(2,1)S(1)} %multiply_convert_fusion.hidden_ref, bf16[896,2048]{1,0:T(8,128)(2,1)} %bitcast.19, bf16[512,512]{1,0:T(8,128)(2,1)S(1)} %get-tuple-element.5.mixed_ref, bf16[512,2048]{1,0:T(8,128)(2,1)S(1)} %copy-done, ...), custom_call_target="tpu_custom_call" | custom-call | flops 20000000000 | bytes 10000000 | tf_op jit(solution)/shard_map/pallas_call | solution.py:541
  93.3 0.8 copy.31
  94.0 0.7 copy.32
  (2 shorter events, 0.0 us)
Async XLA Ops:
  0.6 6.8 %copy-start.7 = (f32[512]{0:T(512)S(1)}, f32[512]{0:T(512)}, u32[]{:S(2)}) copy-start(f32[512]{0:T(512)} %param.21) | copy-start | bytes 6148
  0.6 6.8 %copy-start.1 = (bf16[512,512]{1,0:T(8,128)(2,1)S(1)}, bf16[512,512]{1,0:T(8,128)(2,1)}, u32[]{:S(2)}) copy-start(bf16[512,512]{1,0:T(8,128)(2,1)} %q_ref.1) | copy-start | bytes 1572868
  0.7 6.8 %copy-start.2 = (bf16[512,512]{1,0:T(8,128)(2,1)S(1)}, bf16[512,512]{1,0:T(8,128)(2,1)}, u32[]{:S(2)}) copy-start(bf16[512,512]{1,0:T(8,128)(2,1)} %xf_ref.1) | copy-start | bytes 1572868
  0.7 6.8 %copy-start.3 = (bf16[512,512]{1,0:T(8,128)(2,1)S(1)}, bf16[512,512]{1,0:T(8,128)(2,1)}, u32[]{:S(2)}) copy-start(bf16[512,512]{1,0:T(8,128)(2,1)} %xb_ref.1) | copy-start | bytes 1572868
  0.7 6.8 %copy-start.4 = (bf16[512,512]{1,0:T(8,128)(2,1)S(1)}, bf16[512,512]{1,0:T(8,128)(2,1)}, u32[]{:S(2)}) copy-start(bf16[512,512]{1,0:T(8,128)(2,1)} %v_ref.1) | copy-start | bytes 1572868
  0.7 6.8 %copy-start.6 = (f32[2,512]{1,0:T(2,128)S(1)}, f32[2,512]{1,0:T(2,128)}, u32[]{:S(2)}) copy-start(f32[2,512]{1,0:T(2,128)} %bound_ref.1) | copy-start | bytes 12292
  0.7 6.8 %copy-start.5 = (f32[4,512]{1,0:T(4,128)S(1)}, f32[4,512]{1,0:T(4,128)}, u32[]{:S(2)}) copy-start(f32[4,512]{1,0:T(4,128)} %spike_ref.1) | copy-start | bytes 24580
  7.5 40.5 %copy-start.9 = (bf16[1,2048,896]{2,1,0:T(8,128)(2,1)S(1)}, bf16[1,2048,896]{2,1,0:T(8,128)(2,1)}, u32[]{:S(2)}) copy-start(bf16[1,2048,896]{2,1,0:T(8,128)(2,1)} %param.27) | copy-start | bytes 11010052
  48.0 2.3 %copy-start.10 = (bf16[1,2048,896]{2,1,0:T(8,128)(2,1)S(1)}, bf16[1,2048,896]{2,1,0:T(8,128)(2,1)}, u32[]{:S(2)}) copy-start(bf16[1,2048,896]{2,1,0:T(8,128)(2,1)} %param.28) | copy-start | bytes 11010052
  50.4 2.5 %copy-start.8 = (f32[128,2]{0,1:T(2,128)S(1)}, f32[128,2]{0,1:T(2,128)}, u32[]{:S(2)}) copy-start(f32[128,2]{0,1:T(2,128)} %param.26) | copy-start | bytes 3076
  50.4 2.6 %copy-start = (bf16[512,2048]{1,0:T(8,128)(2,1)S(1)}, bf16[512,2048]{1,0:T(8,128)(2,1)}, u32[]{:S(2)}) copy-start(bf16[512,2048]{1,0:T(8,128)(2,1)} %emit_ref.1) | copy-start | bytes 6291460
